TPU v7x, 32 devices: a whole 2x2x4 slice. The times are simulated.
32 devices in a mesh: sp: 4 (over z), fs: 4 (over y, core), tp: 2 (over x).
Axes of the slice: x: 2, y: 2, z: 4, core: 2. Of those that a mesh axis runs over, the one named last changes fastest.
Arguments:
- tokens: bfloat16 [8, 2048, 2048], P('fs', ('sp', 'tp')), may hold values from -6 to 6
- norm_gain: float32 [2048], replicated, may hold values from 0.1 to 1.9
- w_pool_in: bfloat16 [2048, 1024], P('fs', 'tp'), may hold values from -0.125 to 0.125
- pool_mix: bfloat16 [8, 128, 128], replicated, may hold values from -0.5 to 0.5
- pool_scale: float32 [1024], replicated, may hold values from 0.1 to 1.9
- w_query: bfloat16 [2048, 1024], P('fs', 'tp'), may hold values from -0.13258252 to 0.13258252
- w_key: bfloat16 [2048, 1024], P('fs', 'tp'), may hold values from -0.508233 to 0.508233
- w_value: bfloat16 [2048, 1024], P('fs', 'tp'), may hold values from -0.125 to 0.125
- gate_cache: float32 [8, 8, 2048], P('fs', 'tp'), may hold values from -258 to 0, as said below
- w_out_pool: bfloat16 [1024, 2048], P('tp', 'fs'), may hold values from -0.125 to 0.125
- w_out_attn: bfloat16 [1024, 2048], P('tp', 'fs'), may hold values from -0.75 to 0.75
Outputs:
- mixed: bfloat16 [8, 2048, 2048], P('fs', ('sp', 'tp'))
Inputs may be any that keep to these rules, and one draw needn't show every extreme that they name: `gate_cache`: each head's values never rise along the positions.
All inputs are finite; a program needn't handle non-finite values.
Results may differ from a plain program's by a relative error of at most 0.014.
Values may be sent and summed in bfloat16 or wider, within the bound.
A program may use at most 128 MiB of HBM per device.

v0:
```python
import jax
import jax.numpy as jnp
from jax import lax
from jax.sharding import PartitionSpec as P

HEAD_DIM = 128
GROUP_WIDTH = 128
norm_eps = 1e-06
widest = 16
masked_score = -1e30


def shifted(x, axis, by):
    length = lax.axis_size(axis)
    pairs = [(i, i + by) for i in range(length) if 0 <= i + by < length]
    return lax.ppermute(x, axis, pairs)


def window_sums(extended):
    outcome = []
    current = extended
    offset = 1
    for doubling in range(4):
        padding = jnp.zeros((offset, extended.shape[1]), jnp.float32)
        current = current + jnp.concatenate([padding, current[:-offset]], axis=0)
        offset = offset * 2
        outcome.append(current[widest - 1 :])
    return outcome


def pool_branch(projected, border, first_group, first_position, mixing, scaling):
    row_count = projected.shape[0]
    channels = projected.shape[1]
    widened = projected.astype(jnp.float32)
    totals = window_sums(jnp.concatenate([border.astype(jnp.float32), widened], axis=0))
    token_positions = first_position + jnp.arange(row_count)
    window_index = (first_group + jnp.arange(channels) // GROUP_WIDTH) % 4
    averaged = jnp.zeros((row_count, channels), jnp.float32)
    for doubling in range(4):
        counted = jnp.minimum(token_positions + 1, 2 ** (doubling + 1)).astype(jnp.float32)
        picked = (window_index == doubling).astype(jnp.float32)
        averaged = averaged + picked[None, :] * totals[doubling] / counted[:, None]
    departure = (averaged - widened).astype(jnp.bfloat16)
    group_count = channels // GROUP_WIDTH
    mixed_rows = jnp.einsum(
        "tgc,gcd->tgd",
        departure.reshape(row_count, group_count, GROUP_WIDTH),
        mixing,
        preferred_element_type=jnp.float32,
    )
    return (mixed_rows.reshape(row_count, channels) * scaling[None, :]).astype(jnp.bfloat16)


def on_device(
    tokens,
    norm_gain,
    w_pool_in,
    pool_mix,
    pool_scale,
    w_query,
    w_key,
    w_value,
    gate_cache,
    w_out_pool,
    w_out_attn,
):
    tp_index = lax.axis_index("tp")
    tp_count = lax.axis_size("tp")
    seq_count = tokens.shape[0]
    own_count = tokens.shape[1]
    token_count = own_count * tp_count
    first_position = lax.axis_index("sp") * token_count
    own_rows = tokens.astype(jnp.float32)
    normed = (
        own_rows
        * lax.rsqrt(jnp.mean(own_rows * own_rows, axis=-1, keepdims=True) + norm_eps)
        * norm_gain[None, None, :]
    ).astype(jnp.bfloat16)
    pool_full, query_full, key_full, value_full, out_pool_full, out_attn_full = (
        lax.all_gather(w_pool_in, "fs", axis=0, tiled=True),
        lax.all_gather(w_query, "fs", axis=0, tiled=True),
        lax.all_gather(w_key, "fs", axis=0, tiled=True),
        lax.all_gather(w_value, "fs", axis=0, tiled=True),
        lax.all_gather(w_out_pool, "fs", axis=1, tiled=True),
        lax.all_gather(w_out_attn, "fs", axis=1, tiled=True),
    )
    pool_cols = w_pool_in.shape[1]
    attn_cols = w_query.shape[1]
    shard_rows = lax.all_gather(normed, "tp", axis=1, tiled=True)
    projected = jnp.concatenate(
        [
            jnp.dot(shard_rows, pool_full, preferred_element_type=jnp.float32).astype(jnp.bfloat16),
            jnp.dot(shard_rows, query_full, preferred_element_type=jnp.float32).astype(
                jnp.bfloat16
            ),
            jnp.dot(shard_rows, key_full, preferred_element_type=jnp.float32).astype(jnp.bfloat16),
            jnp.dot(shard_rows, value_full, preferred_element_type=jnp.float32).astype(
                jnp.bfloat16
            ),
        ],
        axis=2,
    )
    pool_in = projected[:, :, :pool_cols]
    query_proj = projected[:, :, pool_cols : pool_cols + attn_cols]
    key_proj = projected[:, :, pool_cols + attn_cols : pool_cols + 2 * attn_cols]
    value_proj = projected[:, :, pool_cols + 2 * attn_cols :]
    group_local = pool_cols // GROUP_WIDTH
    mixing = lax.dynamic_slice_in_dim(pool_mix, tp_index * group_local, group_local, 0)
    scaling = lax.dynamic_slice_in_dim(pool_scale, tp_index * pool_cols, pool_cols, 0)
    borders = shifted(pool_in[:, token_count - (widest - 1) :], "sp", 1)
    pool_out = jnp.stack(
        [
            pool_branch(
                pool_in[member],
                borders[member],
                tp_index * group_local,
                first_position,
                mixing,
                scaling,
            )
            for member in range(seq_count)
        ],
        axis=0,
    )
    head_count = attn_cols // HEAD_DIM
    query_heads = query_proj.reshape(seq_count, token_count, head_count, HEAD_DIM)
    query_gates = jnp.transpose(
        lax.dynamic_slice_in_dim(gate_cache, first_position, token_count, 2), (0, 2, 1)
    )
    query_positions = first_position + jnp.arange(token_count)
    last_position = first_position + token_count - 1
    score_scale = HEAD_DIM ** (-0.5)
    start_state = (
        jnp.full((seq_count, token_count, head_count), masked_score, jnp.float32),
        jnp.zeros((seq_count, token_count, head_count), jnp.float32),
        jnp.zeros((seq_count, token_count, head_count, HEAD_DIM), jnp.float32),
    )
    key_shard = lax.all_gather(key_proj, "sp", axis=1, tiled=True)
    value_shard = lax.all_gather(value_proj, "sp", axis=1, tiled=True)
    key_total = key_shard.shape[1]
    block_rows = 512

    def one_block(block_state, block_index):
        key_start = block_index * block_rows

        def compute(inner_state):
            running_top, running_sum, running_out = inner_state
            key_block = lax.dynamic_slice_in_dim(key_shard, block_index * block_rows, block_rows, 1)
            value_block = lax.dynamic_slice_in_dim(
                value_shard, block_index * block_rows, block_rows, 1
            )
            key_block = key_block.reshape(seq_count, block_rows, head_count, HEAD_DIM)
            value_block = value_block.reshape(seq_count, block_rows, head_count, HEAD_DIM)
            key_gates = lax.dynamic_slice_in_dim(gate_cache, key_start, block_rows, 2)
            scores = (
                jnp.einsum(
                    "sqhd,skhd->sqhk", query_heads, key_block, preferred_element_type=jnp.float32
                )
                * score_scale
            )
            scores = scores + query_gates[:, :, :, None] - key_gates[:, None, :, :]
            allowed = ((key_start + jnp.arange(block_rows))[None, :] <= query_positions[:, None])[
                None, :, None, :
            ]
            scores = jnp.where(allowed, scores, masked_score)
            new_top = jnp.maximum(running_top, jnp.max(scores, axis=3))
            weights = jnp.where(allowed, jnp.exp(scores - new_top[:, :, :, None]), 0.0)
            shrink = jnp.exp(running_top - new_top)
            running_sum = running_sum * shrink + jnp.sum(weights, axis=3)
            running_out = running_out * shrink[:, :, :, None] + jnp.einsum(
                "sqhk,skhd->sqhd",
                weights.astype(jnp.bfloat16),
                value_block,
                preferred_element_type=jnp.float32,
            )
            return (new_top, running_sum, running_out)

        def unchanged(inner_state):
            return inner_state

        return (lax.cond(key_start <= last_position, compute, unchanged, block_state), None)

    result, unused = lax.scan(one_block, start_state, jnp.arange(key_total // block_rows))
    final_top, final_sum, final_out = result
    attn_out = (
        (final_out / final_sum[:, :, :, None])
        .astype(jnp.bfloat16)
        .reshape(seq_count, token_count, attn_cols)
    )
    pool_flat = jnp.transpose(
        pool_out.reshape(seq_count, tp_count, own_count, pool_cols), (1, 0, 2, 3)
    ).reshape(tp_count * seq_count * own_count, pool_cols)
    attn_flat = jnp.transpose(
        attn_out.reshape(seq_count, tp_count, own_count, attn_cols), (1, 0, 2, 3)
    ).reshape(tp_count * seq_count * own_count, attn_cols)
    summed = lax.psum_scatter(
        (
            jnp.dot(pool_flat, out_pool_full, preferred_element_type=jnp.float32)
            + jnp.dot(attn_flat, out_attn_full, preferred_element_type=jnp.float32)
        ).astype(jnp.bfloat16),
        "tp",
        scatter_dimension=0,
        tiled=True,
    ).astype(jnp.float32)
    return summed.astype(jnp.bfloat16).reshape(seq_count, own_count, summed.shape[1])


def solution(mesh):
    placed = (
        P("fs", ("sp", "tp"), None),
        P(),
        P("fs", "tp"),
        P(),
        P(),
        P("fs", "tp"),
        P("fs", "tp"),
        P("fs", "tp"),
        P("fs", "tp", None),
        P("tp", "fs"),
        P("tp", "fs"),
    )
    return jax.shard_map(
        on_device,
        mesh=mesh,
        in_specs=placed,
        out_specs=P("fs", ("sp", "tp"), None),
        check_vma=False,
    )
```

profile of v0, /device:TPU:0, one launch (start us, length us, event | category | flops | bytes accessed | tf_op | source)
XLA Modules:
  0.0 483.2 jit_solution(8892311270368384525)
XLA Ops:
  6.5 0.7 all-gather.16.cloned.1.call-update
  7.3 2.1 fusion.15
  9.4 1.9 fusion.17
  11.4 0.7 all-gather.22.cloned.1.call-update
  12.1 0.5 all-gather.12.cloned.1.call-update
  12.7 1.0 copy.37
  13.8 0.5 all-gather.14.cloned.1.call-update
  14.4 19.8 %all-gather.16.cloned.1.call-done = bf16[2048,512]{1,0:T(8,128)(2,1)} async-done(((bf16[512,512]{1,0:T(8,128)(2,1)}), bf16[2048,512]{1,0:T(8,128)(2,1)}) %all-gather.16.cloned.1.call-update) | async-done | bytes 2097168 | tf_op jit(solution)/shard_map/all_gather | solution.py:82
  34.2 58.3 %all-gather.10.cloned.1.call-done = bf16[2,512,2048]{2,1,0:T(8,128)(2,1)} async-done(((bf16[2,256,2048]{2,1,0:T(8,128)(2,1)}), bf16[2,512,2048]{2,1,0:T(8,128)(2,1)}) %all-gather.10.cloned.1.call-update) | async-done | bytes 4194320 | tf_op jit(solution)/shard_map/all_gather | solution.py:89
  92.5 6.2 %fusion.29 = bf16[2,512,512]{2,1,0:T(8,128)(2,1)} fusion(bf16[2,512,2048]{2,1,0:T(8,128)(2,1)} %all-gather.10.cloned.1.call-done, bf16[2048,512]{1,0:T(8,128)(2,1)} %all-gather.16.cloned.1.call-done), kind=kOutput, calls=%fused_computation.42 | convolution fusion | flops 2148007936 | bytes 7340032 | tf_op jit(solution)/shard_map/dot_general | solution.py:96
  98.8 17.9 %all-gather.22.cloned.1.call-done = bf16[2048,512]{1,0:T(8,128)(2,1)} async-done(((bf16[512,512]{1,0:T(8,128)(2,1)}), bf16[2048,512]{1,0:T(8,128)(2,1)}) %all-gather.22.cloned.1.call-update) | async-done | bytes 2097168 | tf_op jit(solution)/shard_map/all_gather | solution.py:83
  116.7 6.2 %fusion.35 = bf16[2,512,512]{2,1,0:T(8,128)(2,1)} fusion(bf16[2,512,2048]{2,1,0:T(8,128)(2,1)} %all-gather.10.cloned.1.call-done, bf16[2048,512]{1,0:T(8,128)(2,1)} %all-gather.22.cloned.1.call-done), kind=kOutput, calls=%fused_computation.44 | convolution fusion | flops 2148007936 | bytes 7340032 | tf_op jit(solution)/shard_map/dot_general | solution.py:97
  122.9 0.7 all-gather.26.cloned.1.call-update
  123.7 0.7 dynamic_slice.23
  124.4 16.3 %all-gather.12.cloned.1.call-done = bf16[2048,512]{1,0:T(8,128)(2,1)} async-done(((bf16[512,512]{1,0:T(8,128)(2,1)}), bf16[2048,512]{1,0:T(8,128)(2,1)}) %all-gather.12.cloned.1.call-update) | async-done | bytes 2097168 | tf_op jit(solution)/shard_map/all_gather | solution.py:80
  140.7 5.2 %fusion.26 = bf16[2,512,512]{2,1,0:T(8,128)(2,1)S(1)} fusion(bf16[2,512,2048]{2,1,0:T(8,128)(2,1)} %all-gather.10.cloned.1.call-done, bf16[2048,512]{1,0:T(8,128)(2,1)} %all-gather.12.cloned.1.call-done), kind=kOutput, calls=%fused_computation.41 | convolution fusion | flops 2148007936 | bytes 7340032 | tf_op jit(solution)/shard_map/dot_general | solution.py:92
  145.9 4.0 collective-permute-start
  149.9 14.8 %all-gather.20.cloned.1.call-done = bf16[2048,512]{0,1:T(8,128)(2,1)} async-done(((bf16[512,512]{0,1:T(8,128)(2,1)}), bf16[2048,512]{0,1:T(8,128)(2,1)}) %all-gather.20.cloned.1.call-update) | async-done | bytes 2097168 | tf_op jit(solution)/shard_map/all_gather | solution.py:81
  164.7 6.2 %fusion.32 = bf16[2,512,512]{1,2,0:T(8,128)(2,1)} fusion(bf16[2,512,2048]{2,1,0:T(8,128)(2,1)} %all-gather.10.cloned.1.call-done, bf16[2048,512]{0,1:T(8,128)(2,1)} %all-gather.20.cloned.1.call-done), kind=kOutput, calls=%fused_computation.43 | convolution fusion | flops 2148007936 | bytes 7340032 | tf_op jit(solution)/shard_map/dot_general | solution.py:93
  171.2 2.3 copy.39
  173.5 0.8 fusion.71
  174.6 0.5 fusion.38
  176.3 2.9 fusion.67
  179.6 0.7 reshape.190
  180.2 0.8 copy.34
  181.1 1.4 convolution_bitcast_fusion
  182.5 0.7 reshape.192
  183.2 0.8 copy.36
  184.4 4.3 all-gather.14.cloned.1.call-done
  188.7 7.2 %fusion.79 = f32[1024,2048]{1,0:T(8,128)} fusion(bf16[1024,512]{1,0:T(8,128)(2,1)S(1)} %bitcast.129, bf16[512,2048]{1,0:T(8,128)(2,1)} %all-gather.14.cloned.1.call-done), kind=kOutput, calls=%fused_computation.123 | convolution fusion | flops 2147483648 | bytes 11534336 | tf_op jit(solution)/shard_map/dot_general | solution.py:198
  195.9 75.1 %all-gather.18.cloned.1.call-done = bf16[2,2048,512]{2,1,0:T(8,128)(2,1)} async-done(((bf16[2,512,512]{2,1,0:T(8,128)(2,1)}), bf16[2,2048,512]{2,1,0:T(8,128)(2,1)}) %all-gather.18.cloned.1.call-update) | async-done | bytes 4194320 | tf_op jit(solution)/shard_map/all_gather | solution.py:138
  271.0 6.3 %copy.38 = bf16[2,2048,512]{1,2,0:T(8,128)(2,1)} copy(bf16[2,2048,512]{2,1,0:T(8,128)(2,1)} %all-gather.18.cloned.1.call-done) | data formatting | bytes 8388608
  277.3 74.5 %all-gather.24.cloned.1.call-done = bf16[2,2048,512]{2,1,0:T(8,128)(2,1)} async-done(((bf16[2,512,512]{2,1,0:T(8,128)(2,1)}), bf16[2,2048,512]{2,1,0:T(8,128)(2,1)}) %all-gather.24.cloned.1.call-update) | async-done | bytes 4194320 | tf_op jit(solution)/shard_map/all_gather | solution.py:139
  351.9 6.3 %copy.40 = bf16[2,2048,512]{1,2,0:T(8,128)(2,1)} copy(bf16[2,2048,512]{2,1,0:T(8,128)(2,1)} %all-gather.24.cloned.1.call-done) | data formatting | bytes 8388608
  358.4 1.0 copy-done.3
  359.5 17.2 %while.15 = (s32[]{:T(128)}, f32[2,512,4]{1,2,0:T(4,128)S(1)}, f32[2,512,4]{1,2,0:T(4,128)S(1)}, f32[2,512,4,128]{1,3,2,0:T(8,128)S(1)}, s32[4]{0:T(128)S(1)}, /...) while((s32[]{:T(128)}, f32[2,512,4]{1,2,0:T(4,128)S(1)}, ...), condition=%wide.region_6.7_spmd.clone, body=%wide.region_1.6_spmd.clone.sunk | while | flops 1114907648 | bytes 38154664 | solution.py:183
  359.5 0.6 dynamic_slice.35
  360.7 12.1 %conditional.3 = ((f32[2,512,4]{1,2,0:T(4,128)S(1)}, f32[2,512,4]{1,2,0:T(4,128)S(1)}, f32[2,512,4,128]{1,3,2,0:T(8,128)S(1)})) conditional(s32[]{:T(128)} %convert_element_type.217, (f32[2,512,4]{1,2,0:T(4,128)S(1)}, f32[2,512,4]{1,2,0:T(4,128)S(1)}, f32[2,512,4,128]{1,3,2,0:T(8,128)S(1)}) %tuple.49, (s32[]{:T(128)}, s32[]{:T(128)}, s32[]{:T(128)}, ...), branch_computations={%region_2.2_spmd, %region_3.5_spmd} | conditional | flops 1114907648 | bytes 38152320 | solution.py:181
  361.7 1.7 constant_dynamic-slice_fusion
  363.4 2.6 fusion.6
  366.0 3.2 fusion.5
  369.2 3.5 bitcast_add_fusion.1
  372.8 0.6 dynamic_slice.35
  374.1 0.6 dynamic_slice.35
  375.4 0.6 dynamic_slice.35
  377.3 1.5 copy.46
  378.8 8.4 %add_convert_fusion = bf16[1024,2048]{1,0:T(8,128)(2,1)} fusion(f32[1024,2048]{1,0:T(8,128)} %fusion.79, bf16[1024,512]{1,0:T(8,128)(2,1)S(1)} %bitcast.130, bf16[512,2048]{1,0:T(8,128)(2,1)} %all-gather.26.cloned.1.call-done), kind=kOutput, calls=%fused_computation.22 | convolution fusion | flops 2151677952 | bytes 15728640 | tf_op jit(solution)/shard_map/dot_general | solution.py:199
  387.2 89.2 %reduce-scatter.2.cloned.1.call-done = bf16[512,2048]{1,0:T(8,128)(2,1)} async-done(((bf16[1024,2048]{1,0:T(8,128)(2,1)}), bf16[512,2048]{1,0:T(8,128)(2,1)}) %reduce-scatter.2.cloned.1.call-update) | async-done | bytes 2097168 | tf_op jit(solution)/shard_map/reduce_scatter | solution.py:196
  (72 shorter events, 4.1 us)
Async XLA Ops:
  6.5 172.7 %copy-start = (bf16[8,128,128]{2,1,0:T(8,128)(2,1)S(1)}, bf16[8,128,128]{2,1,0:T(8,128)(2,1)}, u32[]{:S(2)}) copy-start(bf16[8,128,128]{2,1,0:T(8,128)(2,1)} %param.18) | copy-start | bytes 786436
  6.5 2.9 copy-start.2
  6.5 2.9 copy-start.6
  6.5 27.7 %all-gather.16.cloned.1.call-start = ((), (), s32[]{:S(2)}) async-start(), calls=%async_computation.4 | async-start | bytes 2621440 | tf_op jit(solution)/shard_map/all_gather | solution.py:82
  7.3 85.2 %all-gather.10.cloned.1.call-start = ((), (), s32[]{:S(2)}) async-start(), calls=%async_computation.1 | async-start | bytes 6291456 | tf_op jit(solution)/shard_map/all_gather | solution.py:89
  11.3 1.4 copy-start.4
  11.3 105.4 %all-gather.22.cloned.1.call-start = ((), (), s32[]{:S(2)}) async-start(), calls=%async_computation.7 | async-start | bytes 2621440 | tf_op jit(solution)/shard_map/all_gather | solution.py:83
  12.0 128.6 %all-gather.12.cloned.1.call-start = ((), (), s32[]{:S(2)}) async-start(), calls=%async_computation.2 | async-start | bytes 2621440 | tf_op jit(solution)/shard_map/all_gather | solution.py:80
  12.6 152.1 %all-gather.20.cloned.1.call-start = ((), (), s32[]{:S(2)}) async-start(), calls=%async_computation.6 | async-start | bytes 2621440 | tf_op jit(solution)/shard_map/all_gather | solution.py:81
  13.7 175.0 %all-gather.14.cloned.1.call-start = ((), (), s32[]{:S(2)}) async-start(), calls=%async_computation.3 | async-start | bytes 2621440 | tf_op jit(solution)/shard_map/all_gather | solution.py:84
  14.3 256.7 %all-gather.18.cloned.1.call-start = ((), (), s32[]{:S(2)}) async-start(), calls=%async_computation.5 | async-start | bytes 5242880 | tf_op jit(solution)/shard_map/all_gather | solution.py:138
  98.7 25.0 %copy-start.8 = (f32[1024]{0:T(1024)S(1)}, f32[1024]{0:T(1024)}, u32[]{:S(2)}) copy-start(f32[1024]{0:T(1024)} %param.19) | copy-start | bytes 12292
  98.7 25.7 %copy-start.5 = (f32[2,4,2048]{2,1,0:T(4,128)S(1)}, f32[2,4,2048]{2,1,0:T(4,128)}, u32[]{:S(2)}) copy-start(f32[2,4,2048]{2,1,0:T(4,128)} %param.23) | copy-start | bytes 196612
  98.7 253.1 %all-gather.24.cloned.1.call-start = ((), (), s32[]{:S(2)}) async-start(), calls=%async_computation.8 | async-start | bytes 5242880 | tf_op jit(solution)/shard_map/all_gather | solution.py:139
  122.9 255.9 %all-gather.26.cloned.1.call-start = ((), (), s32[]{:S(2)}) async-start(), calls=%async_computation.9 | async-start | bytes 2621440 | tf_op jit(solution)/shard_map/all_gather | solution.py:85
  123.6 352.8 %reduce-scatter.2.cloned.1.call-start = ((), (), s32[]{:S(2)}) async-start(), calls=%async_computation.10 | async-start | bytes 6291456 | tf_op jit(solution)/shard_map/reduce_scatter | solution.py:196
  145.9 27.6 %collective-permute-start = (bf16[2,15,512]{2,1,0:T(8,128)(2,1)S(1)}, bf16[2,15,512]{2,1,0:T(8,128)(2,1)}, u32[]{:S(2)}, u32[]{:S(2)}) collective-permute-start(bf16[2,15,512]{2,1,0:T(8,128)(2,1)S(1)} %slice.84), channel_id=1, source_target_pairs={{0,8},{8,16},{16,24},{1,9},{9,17},{17,25},{2,10},{10,18},{18,26},{... | collective-permute-start | bytes 92168 | tf_op jit(solution)/shard_map/ppermute | solution.py:16
  182.5 1.5 copy-start.7
  358.2 1.3 copy-start.3
  387.2 89.2 %copy-start.1 = (bf16[8,128,128]{2,1,0:T(8,128)(2,1)S(1)}, bf16[8,128,128]{2,1,0:T(8,128)(2,1)}, u32[]{:S(2)}) copy-start(bf16[8,128,128]{2,1,0:T(8,128)(2,1)} %param.18) | copy-start | bytes 786436
Sparse Core Ops, SparseCore 0:
  8.9 25.2 all-gather.15
  35.8 56.7 all-gather.9
  94.1 22.5 all-gather.21
  118.1 22.5 all-gather.11
  142.1 22.5 all-gather.19
  166.1 22.5 all-gather.13
  190.3 80.7 all-gather.17
  272.6 79.2 all-gather.23
  353.4 21.0 all-gather.25
  387.3 89.0 reduce-scatter.1
where the time goes:
time: 484 us; the launch traced here: 483 us
  waiting for transfers between devices  374 us (77%)
  matrix products  47.3 us (10%)
  local copies, waits for them, and re-layouts  27 us (6%)
  other arithmetic  13.8 us (3%)
  between operations  13.8 us (3%)
    reduce_scatter x1, waiting for transfers between devices, on_device(): lax.psum_scatter((jnp.dot(pool_flat, out_pool_full, preferred_element_typ...  89.2 us
    all_gather x1, waiting for transfers between devices, on_device(): key_shard = lax.all_gather(key_proj, 'sp', axis=1, tiled=True)  75.1 us
    all_gather x1, waiting for transfers between devices, on_device(): value_shard = lax.all_gather(value_proj, 'sp', axis=1, tiled=True)  74.5 us
    all_gather x1, waiting for transfers between devices, on_device(): shard_rows = lax.all_gather(normed, 'tp', axis=1, tiled=True)  58.3 us
    all_gather x1, waiting for transfers between devices, on_device(): lax.all_gather(w_key, 'fs', axis=0, tiled=True)  19.8 us
    all_gather x1, waiting for transfers between devices, on_device(): lax.all_gather(w_value, 'fs', axis=0, tiled=True)  17.9 us
    unnamed x22, local copies, waits for them, and re-layouts  17 us
    all_gather x1, waiting for transfers between devices, on_device(): lax.all_gather(w_pool_in, 'fs', axis=0, tiled=True)  16.3 us
  transfers between devices with their start and end apart: 11, of which 9 were waited for; matrix products, arithmetic and copies ran while one was open for 16% of the time, Pallas kernels for 0%

commit v1 on v0

--- a/solution.py
+++ b/solution.py
@@ -8,6 +8,17 @@
 norm_eps = 1e-06
 widest = 16
 masked_score = -1e30
+
+
+def turned_line(block, axis, dim):
+    size = lax.axis_size(axis)
+    right = [(i, (i + 1) % size) for i in range(size)]
+    parts = [block]
+    for stride in range(1, size):
+        parts = [lax.ppermute(parts[0], axis, right), *parts]
+    whole = jnp.concatenate(parts, axis=dim)
+    shift = (lax.axis_index(axis) + 1) * parts[-1].shape[dim]
+    return jnp.roll(whole, shift, axis=dim)
 
 
 def shifted(x, axis, by):
@@ -136,7 +147,7 @@
         jnp.zeros((seq_count, token_count, head_count, HEAD_DIM), jnp.float32),
     )
     key_shard = lax.all_gather(key_proj, "sp", axis=1, tiled=True)
-    value_shard = lax.all_gather(value_proj, "sp", axis=1, tiled=True)
+    value_shard = turned_line(value_proj, "sp", 1)
     key_total = key_shard.shape[1]
     block_rows = 512
 

time: 484 us -> 427 us (0.88)
  waiting for transfers between devices: 374 us -> 298 us
  local copies, waits for them, and re-layouts: 27 us -> 40.8 us
  starting transfers between devices: 4.34 us -> 9.66 us
    all_gather x1 -> x0, waiting for transfers between devices: 74.5 us -> none  [on_device(): value_shard = lax.all_gather(value_proj, 'sp', axis=1, tiled=True)]
    ppermute x0 -> x3, waiting for transfers between devices: none -> 57.6 us  [turned_line(): parts = [lax.ppermute(parts[0], axis, right), *parts]]
    all_gather x1, waiting for transfers between devices: 75.1 us -> 22.1 us  [on_device(): key_shard = lax.all_gather(key_proj, 'sp', axis=1, tiled=True)]
    unnamed x22 -> x35, local copies, waits for them, and re-layouts: 17 us -> 24.3 us
    ppermute x0 -> x3, starting transfers between devices: none -> 5.36 us  [turned_line(): parts = [lax.ppermute(parts[0], axis, right), *parts]]
  transfers between devices with their start and end apart: 11 -> 13, of which waited for: 9 -> 9; matrix products, arithmetic and copies ran while one was open for 16% -> 21% of each run, Pallas kernels for 0% -> 0%
where the time goes in v1:
time: 427 us; the launch traced here: 426 us
  waiting for transfers between devices  298 us (70%)
  matrix products  46.3 us (11%)
  local copies, waits for them, and re-layouts  40.8 us (10%)
  other arithmetic  14.2 us (3%)
  between operations  13.6 us (3%)
  starting transfers between devices  9.66 us (2%)
    reduce_scatter x1, waiting for transfers between devices, on_device(): lax.psum_scatter((jnp.dot(pool_flat, out_pool_full, preferred_element_typ...  89.5 us
    all_gather x1, waiting for transfers between devices, on_device(): shard_rows = lax.all_gather(normed, 'tp', axis=1, tiled=True)  58.3 us
    ppermute x3, waiting for transfers between devices, turned_line(): parts = [lax.ppermute(parts[0], axis, right), *parts]  57.6 us
    unnamed x35, local copies, waits for them, and re-layouts  24.3 us
    all_gather x1, waiting for transfers between devices, on_device(): key_shard = lax.all_gather(key_proj, 'sp', axis=1, tiled=True)  22.1 us
    all_gather x1, waiting for transfers between devices, on_device(): lax.all_gather(w_key, 'fs', axis=0, tiled=True)  19.9 us
    all_gather x1, waiting for transfers between devices, on_device(): lax.all_gather(w_value, 'fs', axis=0, tiled=True)  18.5 us
    all_gather x1, waiting for transfers between devices, on_device(): lax.all_gather(w_pool_in, 'fs', axis=0, tiled=True)  16.4 us
  transfers between devices with their start and end apart: 13, of which 9 were waited for; matrix products, arithmetic and copies ran while one was open for 21% of the time, Pallas kernels for 0%

profile of v1, /device:TPU:0, one launch (start us, length us, event | category | flops | bytes accessed | tf_op | source)
XLA Modules:
  0.0 425.9 jit_solution(4818338535322762356)
XLA Ops:
  6.5 0.7 all-gather.15.cloned.1.call-update
  7.3 2.1 fusion.15
  9.4 1.9 fusion.17
  12.7 1.0 copy.37
  14.4 19.9 %all-gather.15.cloned.1.call-done = bf16[2048,512]{1,0:T(8,128)(2,1)} async-done(((bf16[512,512]{1,0:T(8,128)(2,1)}), bf16[2048,512]{1,0:T(8,128)(2,1)}) %all-gather.15.cloned.1.call-update) | async-done | bytes 2097168 | tf_op jit(solution)/shard_map/all_gather | solution.py:93
  34.2 58.3 %all-gather.9.cloned.1.call-done = bf16[2,512,2048]{2,1,0:T(8,128)(2,1)} async-done(((bf16[2,256,2048]{2,1,0:T(8,128)(2,1)}), bf16[2,512,2048]{2,1,0:T(8,128)(2,1)}) %all-gather.9.cloned.1.call-update) | async-done | bytes 4194320 | tf_op jit(solution)/shard_map/all_gather | solution.py:100
  92.5 6.2 %fusion.29 = bf16[2,512,512]{2,1,0:T(8,128)(2,1)} fusion(bf16[2,512,2048]{2,1,0:T(8,128)(2,1)} %all-gather.9.cloned.1.call-done, bf16[2048,512]{1,0:T(8,128)(2,1)} %all-gather.15.cloned.1.call-done), kind=kOutput, calls=%fused_computation.42 | convolution fusion | flops 2148007936 | bytes 7340032 | tf_op jit(solution)/shard_map/dot_general | solution.py:107
  100.3 16.4 %all-gather.11.cloned.1.call-done = bf16[2048,512]{1,0:T(8,128)(2,1)} async-done(((bf16[512,512]{1,0:T(8,128)(2,1)}), bf16[2048,512]{1,0:T(8,128)(2,1)}) %all-gather.11.cloned.1.call-update) | async-done | bytes 2097168 | tf_op jit(solution)/shard_map/all_gather | solution.py:91
  116.7 5.2 %fusion.26 = bf16[2,512,512]{2,1,0:T(8,128)(2,1)S(1)} fusion(bf16[2,512,2048]{2,1,0:T(8,128)(2,1)} %all-gather.9.cloned.1.call-done, bf16[2048,512]{1,0:T(8,128)(2,1)} %all-gather.11.cloned.1.call-done), kind=kOutput, calls=%fused_computation.41 | convolution fusion | flops 2148007936 | bytes 7340032 | tf_op jit(solution)/shard_map/dot_general | solution.py:103
  122.2 18.5 %all-gather.21.cloned.1.call-done = bf16[2048,512]{1,0:T(8,128)(2,1)} async-done(((bf16[512,512]{1,0:T(8,128)(2,1)}), bf16[2048,512]{1,0:T(8,128)(2,1)}) %all-gather.21.cloned.1.call-update) | async-done | bytes 2097168 | tf_op jit(solution)/shard_map/all_gather | solution.py:94
  140.7 6.2 %fusion.35 = bf16[2,512,512]{2,1,0:T(8,128)(2,1)} fusion(bf16[2,512,2048]{2,1,0:T(8,128)(2,1)} %all-gather.9.cloned.1.call-done, bf16[2048,512]{1,0:T(8,128)(2,1)} %all-gather.21.cloned.1.call-done), kind=kOutput, calls=%fused_computation.44 | convolution fusion | flops 2148007936 | bytes 7340032 | tf_op jit(solution)/shard_map/dot_general | solution.py:108
  146.9 1.5 collective-permute-start.1
  148.4 4.0 collective-permute-start
  152.4 12.3 %all-gather.19.cloned.1.call-done = bf16[2048,512]{0,1:T(8,128)(2,1)} async-done(((bf16[512,512]{0,1:T(8,128)(2,1)}), bf16[2048,512]{0,1:T(8,128)(2,1)}) %all-gather.19.cloned.1.call-update) | async-done | bytes 2097168 | tf_op jit(solution)/shard_map/all_gather | solution.py:92
  164.7 6.2 %fusion.32 = bf16[2,512,512]{1,2,0:T(8,128)(2,1)} fusion(bf16[2,512,2048]{2,1,0:T(8,128)(2,1)} %all-gather.9.cloned.1.call-done, bf16[2048,512]{0,1:T(8,128)(2,1)} %all-gather.19.cloned.1.call-done), kind=kOutput, calls=%fused_computation.43 | convolution fusion | flops 2148007936 | bytes 7340032 | tf_op jit(solution)/shard_map/dot_general | solution.py:104
  170.9 2.3 copy.39
  173.2 0.7 fusion.71
  175.5 0.7 copy-done.2
  176.6 1.7 collective-permute-start.2
  178.3 2.2 fusion.67
  180.8 25.2 %collective-permute-done.2 = bf16[2,512,512]{2,1,0:T(8,128)(2,1)} collective-permute-done((bf16[2,512,512]{2,1,0:T(8,128)(2,1)}, bf16[2,512,512]{2,1,0:T(8,128)(2,1)}, u32[]{:S(2)}, u32[]{:S(2)}) %collective-permute-start.2) | collective-permute-done | bytes 1048608 | tf_op jit(solution)/shard_map/ppermute | solution.py:18
  206.1 2.2 collective-permute-start.3
  208.6 1.6 reshape.192
  210.2 2.3 copy.36
  213.2 1.6 copy.34
  214.8 1.5 multiply_convert_fusion.1
  216.4 7.3 %fusion.79 = f32[1024,2048]{1,0:T(8,128)} fusion(bf16[1024,512]{1,0:T(8,128)(2,1)S(1)} %bitcast.129, bf16[512,2048]{1,0:T(8,128)(2,1)} %all-gather.13.cloned.1.call-done), kind=kOutput, calls=%fused_computation.132 | convolution fusion | flops 2147483648 | bytes 11534336 | tf_op jit(solution)/shard_map/dot_general | solution.py:209
  223.7 32.4 %collective-permute-done.3 = bf16[2,512,512]{2,1,0:T(8,128)(2,1)S(1)} collective-permute-done((bf16[2,512,512]{2,1,0:T(8,128)(2,1)}, bf16[2,512,512]{2,1,0:T(8,128)(2,1)S(1)}, u32[]{:S(2)}, u32[]{:S(2)}) %collective-permute-start.3) | collective-permute-done | bytes 1048608 | tf_op jit(solution)/shard_map/ppermute | solution.py:18
  256.2 1.3 constant_dynamic-update-slice_fusion.6
  257.5 1.3 constant_dynamic-update-slice_fusion.5
  258.8 1.3 constant_dynamic-update-slice_fusion.4
  260.2 1.3 constant_dynamic-update-slice_fusion.2
  261.5 1.3 constant_dynamic-update-slice_fusion.1
  262.8 1.3 constant_dynamic-update-slice_fusion
  264.1 2.2 constant_dynamic-slice_fusion.3
  266.3 6.3 %copy.40 = bf16[2,2048,512]{1,2,0:T(8,128)(2,1)} copy(bf16[2,2048,512]{2,1,0:T(8,128)(2,1)} %constant_dynamic-slice_fusion.3) | data formatting | bytes 8388608
  272.6 22.1 %all-gather.17.cloned.1.call-done = bf16[2,2048,512]{2,1,0:T(8,128)(2,1)} async-done(((bf16[2,512,512]{2,1,0:T(8,128)(2,1)}), bf16[2,2048,512]{2,1,0:T(8,128)(2,1)}) %all-gather.17.cloned.1.call-update) | async-done | bytes 4194320 | tf_op jit(solution)/shard_map/all_gather | solution.py:149
  294.7 6.2 %copy.38 = bf16[2,2048,512]{1,2,0:T(8,128)(2,1)} copy(bf16[2,2048,512]{2,1,0:T(8,128)(2,1)} %all-gather.17.cloned.1.call-done) | data formatting | bytes 8388608
  301.2 1.0 copy-done.6
  302.2 17.2 %while.15 = (s32[]{:T(128)}, f32[2,512,4]{1,2,0:T(4,128)S(1)}, f32[2,512,4]{1,2,0:T(4,128)S(1)}, f32[2,512,4,128]{1,3,2,0:T(8,128)S(1)}, s32[4]{0:T(128)S(1)}, /...) while((s32[]{:T(128)}, f32[2,512,4]{1,2,0:T(4,128)S(1)}, ...), condition=%wide.region_6.7_spmd.clone, body=%wide.region_1.6_spmd.clone.sunk | while | flops 1114907648 | bytes 38154656 | solution.py:194
  303.5 12.0 %conditional.3 = ((f32[2,512,4]{1,2,0:T(4,128)S(1)}, f32[2,512,4]{1,2,0:T(4,128)S(1)}, f32[2,512,4,128]{1,3,2,0:T(8,128)S(1)})) conditional(s32[]{:T(128)} %convert_element_type.217, (f32[2,512,4]{1,2,0:T(4,128)S(1)}, f32[2,512,4]{1,2,0:T(4,128)S(1)}, f32[2,512,4,128]{1,3,2,0:T(8,128)S(1)}) %tuple.49, (s32[]{:T(128)}, s32[]{:T(128)}, s32[]{:T(128)}, ...), branch_computations={%region_2.2_spmd, %region_3.5_spmd} | conditional | flops 1114907648 | bytes 38152320 | solution.py:192
  304.4 1.7 constant_dynamic-slice_fusion
  306.1 2.6 fusion.6
  308.8 3.2 fusion.5
  312.0 3.5 bitcast_add_fusion.1
  320.0 1.5 copy.46
  321.5 8.4 %add_convert_fusion = bf16[1024,2048]{1,0:T(8,128)(2,1)} fusion(f32[1024,2048]{1,0:T(8,128)} %fusion.79, bf16[1024,512]{1,0:T(8,128)(2,1)S(1)} %bitcast.130, bf16[512,2048]{1,0:T(8,128)(2,1)} %all-gather.23.cloned.1.call-done), kind=kOutput, calls=%fused_computation.22 | convolution fusion | flops 2151677952 | bytes 15728640 | tf_op jit(solution)/shard_map/dot_general | solution.py:210
  329.9 89.5 %reduce-scatter.2.cloned.1.call-done = bf16[512,2048]{1,0:T(8,128)(2,1)} async-done(((bf16[1024,2048]{1,0:T(8,128)(2,1)}), bf16[512,2048]{1,0:T(8,128)(2,1)}) %reduce-scatter.2.cloned.1.call-update) | async-done | bytes 2097168 | tf_op jit(solution)/shard_map/reduce_scatter | solution.py:207
  (91 shorter events, 10.9 us)
Async XLA Ops:
  6.5 173.9 %copy-start = (bf16[8,128,128]{2,1,0:T(8,128)(2,1)S(1)}, bf16[8,128,128]{2,1,0:T(8,128)(2,1)}, u32[]{:S(2)}) copy-start(bf16[8,128,128]{2,1,0:T(8,128)(2,1)} %param.18) | copy-start | bytes 786436
  6.5 2.9 copy-start.4
  6.5 2.9 copy-start.9
  6.5 27.7 %all-gather.15.cloned.1.call-start = ((), (), s32[]{:S(2)}) async-start(), calls=%async_computation.4 | async-start | bytes 2621440 | tf_op jit(solution)/shard_map/all_gather | solution.py:93
  7.3 85.2 %all-gather.9.cloned.1.call-start = ((), (), s32[]{:S(2)}) async-start(), calls=%async_computation.1 | async-start | bytes 6291456 | tf_op jit(solution)/shard_map/all_gather | solution.py:100
  11.3 1.4 copy-start.7
  11.3 105.4 %all-gather.11.cloned.1.call-start = ((), (), s32[]{:S(2)}) async-start(), calls=%async_computation.2 | async-start | bytes 2621440 | tf_op jit(solution)/shard_map/all_gather | solution.py:91
  12.0 128.6 %all-gather.21.cloned.1.call-start = ((), (), s32[]{:S(2)}) async-start(), calls=%async_computation.7 | async-start | bytes 2621440 | tf_op jit(solution)/shard_map/all_gather | solution.py:94
  12.6 152.1 %all-gather.19.cloned.1.call-start = ((), (), s32[]{:S(2)}) async-start(), calls=%async_computation.6 | async-start | bytes 2621440 | tf_op jit(solution)/shard_map/all_gather | solution.py:92
  13.7 202.7 %all-gather.13.cloned.1.call-start = ((), (), s32[]{:S(2)}) async-start(), calls=%async_computation.3 | async-start | bytes 2621440 | tf_op jit(solution)/shard_map/all_gather | solution.py:95
  14.3 85.3 %copy-start.8 = (f32[2,4,2048]{2,1,0:T(4,128)S(1)}, f32[2,4,2048]{2,1,0:T(4,128)}, u32[]{:S(2)}) copy-start(f32[2,4,2048]{2,1,0:T(4,128)} %param.23) | copy-start | bytes 196612
  14.3 85.4 %copy-start.11 = (f32[1024]{0:T(1024)S(1)}, f32[1024]{0:T(1024)}, u32[]{:S(2)}) copy-start(f32[1024]{0:T(1024)} %param.19) | copy-start | bytes 12292
  14.3 280.4 %all-gather.17.cloned.1.call-start = ((), (), s32[]{:S(2)}) async-start(), calls=%async_computation.5 | async-start | bytes 5242880 | tf_op jit(solution)/shard_map/all_gather | solution.py:149
  98.7 222.7 %all-gather.23.cloned.1.call-start = ((), (), s32[]{:S(2)}) async-start(), calls=%async_computation.8 | async-start | bytes 2621440 | tf_op jit(solution)/shard_map/all_gather | solution.py:96
  99.5 319.9 %reduce-scatter.2.cloned.1.call-start = ((), (), s32[]{:S(2)}) async-start(), calls=%async_computation.9 | async-start | bytes 6291456 | tf_op jit(solution)/shard_map/reduce_scatter | solution.py:207
  146.9 29.7 %collective-permute-start.1 = (bf16[2,512,512]{2,1,0:T(8,128)(2,1)}, bf16[2,512,512]{2,1,0:T(8,128)(2,1)}, u32[]{:S(2)}, u32[]{:S(2)}) collective-permute-start(bf16[2,512,512]{2,1,0:T(8,128)(2,1)} %fusion.35), channel_id=1, source_target_pairs={{0,8},{8,16},{16,24},{24,0},{1,9},{9,17},{17,25},{25,1},{2,10},{10... | collective-permute-start | bytes 3145736 | tf_op jit(solution)/shard_map/ppermute | solution.py:18
  148.4 24.8 %collective-permute-start = (bf16[2,15,512]{2,1,0:T(8,128)(2,1)S(1)}, bf16[2,15,512]{2,1,0:T(8,128)(2,1)}, u32[]{:S(2)}, u32[]{:S(2)}) collective-permute-start(bf16[2,15,512]{2,1,0:T(8,128)(2,1)S(1)} %slice.84), channel_id=1, source_target_pairs={{0,8},{8,16},{16,24},{1,9},{9,17},{17,25},{2,10},{10,18},{18,26},{... | collective-permute-start | bytes 92168 | tf_op jit(solution)/shard_map/ppermute | solution.py:27
  175.3 1.0 copy-start.2
  176.3 2.0 copy-start.3
  176.3 2.0 slice-start
  176.6 29.5 %collective-permute-start.2 = (bf16[2,512,512]{2,1,0:T(8,128)(2,1)}, bf16[2,512,512]{2,1,0:T(8,128)(2,1)}, u32[]{:S(2)}, u32[]{:S(2)}) collective-permute-start(bf16[2,512,512]{2,1,0:T(8,128)(2,1)} %collective-permute-done.1), channel_id=1, source_target_pairs={{0,8},{8,16},{16,24},{24,0},{1,9},{9,17},{17,25},{25,1},{2,10},{10... | collective-permute-start | bytes 3145736 | tf_op jit(solution)/shard_map/ppermute | solution.py:18
  206.1 50.0 %collective-permute-start.3 = (bf16[2,512,512]{2,1,0:T(8,128)(2,1)}, bf16[2,512,512]{2,1,0:T(8,128)(2,1)S(1)}, u32[]{:S(2)}, u32[]{:S(2)}) collective-permute-start(bf16[2,512,512]{2,1,0:T(8,128)(2,1)} %collective-permute-done.2), channel_id=1, source_target_pairs={{0,8},{8,16},{16,24},{24,0},{1,9},{9,17},{17,25},{25,1},{2,10},{10... | collective-permute-start | bytes 3145736 | tf_op jit(solution)/shard_map/ppermute | solution.py:18
  212.5 2.3 copy-start.10
  213.2 1.6 copy-start.5
  300.9 1.3 copy-start.6
  329.9 89.5 %copy-start.1 = (bf16[8,128,128]{2,1,0:T(8,128)(2,1)S(1)}, bf16[8,128,128]{2,1,0:T(8,128)(2,1)}, u32[]{:S(2)}) copy-start(bf16[8,128,128]{2,1,0:T(8,128)(2,1)} %param.18) | copy-start | bytes 786436
Sparse Core Ops, SparseCore 0:
  8.9 25.2 all-gather.14
  35.8 56.7 all-gather.8
  94.1 22.5 all-gather.10
  118.1 22.5 all-gather.20
  142.1 22.5 all-gather.18
  166.1 22.5 all-gather.12
  190.3 104.3 all-gather.16
  296.2 20.4 all-gather.22
  330.1 89.2 reduce-scatter.1
